TPU v7x, 256 devices: a 4x2x16 block of a 4x16x16 slice. The times are simulated.
256 devices in a mesh: grp: 2 (over y), ep: 32 (over z, core), tp: 4 (over x).
Axes of the slice: x: 4, y: 2, z: 16, core: 2. Of those that a mesh axis runs over, the one named last changes fastest.
The devices are a block of a 4x16x16 slice.
Arguments:
- queries: bfloat16 [24576, 1024], P(('grp', 'ep'), 'tp'), parts along dimension 0, may hold values from -6 to 6
- key_values: bfloat16 [24576, 512], P(('grp', 'ep'), 'tp'), parts along dimension 0, may hold values from -6 to 6
- query_gain: float32 [64], replicated, may hold values from 0.5 to 5
- key_gain: float32 [64], replicated, may hold values from 0.5 to 5
- out_weight: bfloat16 [1024, 2048], P('tp'), may hold values from -0.1875 to 0.1875
- second_batch: bfloat16 [32768, 2048], P(('grp', 'ep', 'tp')), parts along dimension 0, may hold values from -6 to 6
- norm_gain: float32 [2048], replicated, may hold values from 0.1 to 1.9
- routes: int32 [32768, 2], P(('grp', 'ep', 'tp')), parts along dimension 0, may hold values from 0 to 63, all different within a row; in each aligned block of 128 rows (0 to 127, 128 to 255, ...) at most 6 rows name the same one
- route_weights: float32 [32768, 2], P(('grp', 'ep', 'tp')), parts along dimension 0, may hold values from 0.2 to 1
- expert_gate: bfloat16 [64, 2048, 1024], P('ep', None, 'tp'), may hold values from -0.125 to 0.125
- expert_up: bfloat16 [64, 2048, 1024], P('ep', None, 'tp'), may hold values from -0.125 to 0.125
- expert_down: bfloat16 [64, 1024, 2048], P('ep', 'tp'), may hold values from -0.1875 to 0.1875
- shared_gate: bfloat16 [2048, 512], P(None, 'tp'), may hold values from -0.125 to 0.125
- shared_up: bfloat16 [2048, 512], P(None, 'tp'), may hold values from -0.125 to 0.125
- shared_down: bfloat16 [512, 2048], P('tp'), may hold values from -0.25 to 0.25
Outputs:
- mixer_out: bfloat16 [24576, 2048], P(('grp', 'ep', 'tp')), parts along dimension 0
- channel_out: bfloat16 [32768, 2048], P(('grp', 'ep', 'tp')), parts along dimension 0
There are 2 independent parts, one for each index of `grp`. A program takes and returns all parts, laid end to end along the dimension named above; an argument that names none is the same for every part. Nothing has to cross between parts.
Inputs may be any that keep to these rules, and one draw needn't show every extreme that they name: `routes`: each row names 2 different experts. Among the rows of one device no expert is named more than 6 times, and in every draw some expert is named exactly 6 times by the rows of some device.
All inputs are finite; a program needn't handle non-finite values.
Results may differ from a plain program's by a relative error of at most 0.015.
The roundings to bfloat16 on the way count: a program that leaves them out, or rounds other values in their place, can miss the bound.
Values may be sent and summed in bfloat16 or wider, within the bound.
A program may use at most 128 MiB of HBM per device.

v0:
```python
import jax
import jax.numpy as jnp
from jax import lax
from jax.sharding import Mesh
from jax.sharding import PartitionSpec as P

GRID_W = 64
EP = ("ep_0", "ep_1")
GRP_EP = ("grp", "ep_0", "ep_1")
GRP_EP_TP = ("grp", "ep_0", "ep_1", "tp")
rope_base = 10000.0
norm_eps = 1e-06


def joined_along(tiles, dim):
    shape = list(tiles.shape[1:])
    shape[dim] *= tiles.shape[0]
    return jnp.moveaxis(tiles, 0, dim).reshape(shape)


def stacked_from(shard, axes, order):
    tiles = shard
    for k in order:
        tiles = lax.all_gather(tiles, axes[k])
    done = order[::-1]
    back = [done.index(k) for k in range(len(axes))]
    tiles = tiles.transpose(*back, *range(len(axes), tiles.ndim))
    return tiles.reshape(-1, *shard.shape)


def whole_of(shard, axes, order, dim):
    return joined_along(stacked_from(shard, axes, order), dim)


def from_everyone(shard, axis):
    copies = jnp.broadcast_to(shard, (lax.axis_size(axis), *shard.shape))
    return lax.all_to_all(copies, axis, split_axis=0, concat_axis=0, tiled=True)


def gathered_copies(shard, axis, dim):
    return joined_along(from_everyone(shard, axis), dim)


def in_blocks(shard, dim, length):
    shape = shard.shape
    tiles = shard.reshape(*shape[:dim], length, shape[dim] // length, *shape[dim + 1 :])
    return jnp.moveaxis(tiles, dim, 0)


def summed_on_arrival(shard, axis, dim):
    tiles = in_blocks(shard, dim, lax.axis_size(axis))
    arrived = lax.all_to_all(tiles, axis, split_axis=0, concat_axis=0, tiled=True)
    return arrived.astype(jnp.float32).sum(axis=0)


def head_norm(vectors, gain):
    return (
        vectors * lax.rsqrt(jnp.mean(vectors * vectors, axis=-1, keepdims=True) + norm_eps) * gain
    )


def turn_heads(vectors, positions):
    row_count, head_count, head_size = vectors.shape
    half_size = head_size // 2
    inverse = rope_base ** (-jnp.arange(0, half_size, 2, dtype=jnp.float32) / half_size)
    grid_row = (positions // GRID_W).astype(jnp.float32)
    grid_column = (positions % GRID_W).astype(jnp.float32)
    angles = jnp.concatenate([grid_row[:, None] * inverse, grid_column[:, None] * inverse], axis=-1)
    cosine = jnp.cos(angles)[:, None, :]
    sine = jnp.sin(angles)[:, None, :]
    paired = vectors.reshape(row_count, head_count, half_size, 2)
    first = paired[..., 0]
    second = paired[..., 1]
    turned = jnp.stack([first * cosine - second * sine, first * sine + second * cosine], axis=-1)
    return turned.reshape(vectors.shape)


def slot_ids(route_rows, expert_count, capacity):
    row_count, top_count = route_rows.shape
    flat_routes = route_rows.reshape(-1)
    onehot = (flat_routes[:, None] == jnp.arange(expert_count, dtype=jnp.int32)[None, :]).astype(
        jnp.int32
    )
    earlier = jnp.cumsum(onehot, axis=0) - onehot
    within = jnp.sum(earlier * onehot, axis=1)
    return (flat_routes * capacity + within).reshape(row_count, top_count)


def slot_table(slots, slot_count):
    row_count, top_count = slots.shape
    flat_slots = slots.reshape(-1)
    owner_row = jnp.arange(row_count * top_count, dtype=jnp.int32) // top_count
    matches = flat_slots[None, :] == jnp.arange(slot_count, dtype=jnp.int32)[:, None]
    occupied = jnp.any(matches, axis=1)
    source_row = jnp.sum(jnp.where(matches, owner_row[None, :], 0), axis=1)
    return jnp.where(occupied, source_row, row_count)


def pick_block(row_count):
    for candidate in range(min(row_count, 1024), 0, -1):
        if row_count % candidate == 0:
            return candidate
    return row_count


def attend_keys(query_turned, scale, running, pieces):
    head_size = query_turned.shape[-1]
    key_block = pick_block(pieces.shape[0])
    blocks = pieces.reshape(pieces.shape[0] // key_block, key_block, 2 * head_size)

    def one_block(carried, block_rows):
        top_now, total_now, acc_now = carried
        scores = (
            jnp.einsum(
                "qhd,kd->hqk",
                query_turned,
                block_rows[:, :head_size],
                preferred_element_type=jnp.float32,
            )
            * scale
        )
        top_new = jnp.maximum(top_now, jnp.max(scores, axis=-1))
        shrink = jnp.exp(top_now - top_new)
        exps = jnp.exp(scores - top_new[..., None])
        total_new = total_now * shrink + jnp.sum(exps, axis=-1)
        acc_new = acc_now * shrink[..., None] + jnp.einsum(
            "hqk,kd->hqd",
            exps.astype(jnp.bfloat16),
            block_rows[:, head_size:],
            preferred_element_type=jnp.float32,
        )
        return ((top_new, total_new, acc_new), None)

    result, ignored = lax.scan(one_block, running, blocks)
    return result


def shared_hidden_of(token_rows, gate_weights, up_weights):
    gate_part = jnp.dot(token_rows, gate_weights, preferred_element_type=jnp.float32)
    up_part = jnp.dot(token_rows, up_weights, preferred_element_type=jnp.float32)
    return (jax.nn.silu(gate_part) * up_part).astype(jnp.bfloat16)


def expert_hidden(slot_rows, gate_weights, up_weights):
    gate_part = jnp.einsum(
        "osjcd,jdf->osjcf", slot_rows, gate_weights, preferred_element_type=jnp.float32
    )
    up_part = jnp.einsum(
        "osjcd,jdf->osjcf", slot_rows, up_weights, preferred_element_type=jnp.float32
    )
    return (jax.nn.silu(gate_part) * up_part).astype(jnp.bfloat16)


def body(
    queries,
    key_values,
    query_gain,
    key_gain,
    out_weight,
    second_batch,
    norm_gain,
    routes,
    route_weights,
    expert_gate,
    expert_up,
    expert_down,
    shared_gate,
    shared_up,
    shared_down,
):
    query_rows = queries.shape[0]
    head_size = query_gain.shape[0]
    heads_here = queries.shape[1] // head_size
    ep_count = lax.axis_size(EP)
    positions = lax.axis_index(EP) * query_rows + jnp.arange(query_rows, dtype=jnp.int32)
    query_turned = turn_heads(
        head_norm(
            queries.reshape(query_rows, heads_here, head_size).astype(jnp.float32), query_gain
        ),
        positions,
    ).astype(jnp.bfloat16)
    key_turned = turn_heads(
        head_norm(key_values[:, None, :head_size].astype(jnp.float32), key_gain), positions
    ).astype(jnp.bfloat16)
    keys_and_values = jnp.concatenate([key_turned[:, 0, :], key_values[:, head_size:]], axis=1)
    start_state = (
        jnp.full((heads_here, query_rows), -1e30, jnp.float32),
        jnp.zeros((heads_here, query_rows), jnp.float32),
        jnp.zeros((heads_here, query_rows, head_size), jnp.float32),
    )
    top_all, total_all, acc_all = attend_keys(
        query_turned, head_size ** (-0.5), start_state, whole_of(keys_and_values, EP, (0, 1), 0)
    )
    head_out = (
        (acc_all / total_all[..., None])
        .transpose(1, 0, 2)
        .reshape(query_rows, heads_here * head_size)
        .astype(jnp.bfloat16)
    )
    tok_count = second_batch.shape[0]
    model_width = second_batch.shape[1]
    top_count = routes.shape[1]
    local_experts = expert_gate.shape[0]
    expert_count = local_experts * ep_count
    capacity = 3 * tok_count * top_count // (2 * expert_count)
    slot_count = expert_count * capacity
    token_float = second_batch.astype(jnp.float32)
    normed = (
        token_float
        * lax.rsqrt(jnp.mean(token_float * token_float, axis=-1, keepdims=True) + norm_eps)
        * norm_gain
    ).astype(jnp.bfloat16)
    own_slots = slot_ids(routes, expert_count, capacity)
    shared_hidden = (lambda pieces, begin_at: shared_hidden_of(pieces, shared_gate, shared_up))(
        gathered_copies(normed, "tp", 0), jnp.int32(0)
    )
    outgoing = jnp.take(
        normed, slot_table(own_slots, slot_count), axis=0, mode="fill", fill_value=0
    )[None]
    arrived = lax.all_to_all(outgoing, EP, split_axis=1, concat_axis=1, tiled=True)
    arrived = arrived.reshape(arrived.shape[0], ep_count, local_experts, capacity, model_width)
    hidden = expert_hidden(
        lax.all_gather(arrived, "tp", axis=0, tiled=True), expert_gate, expert_up
    )
    routed_part = jnp.einsum(
        "osjcf,jfd->osjcd", hidden, expert_down, preferred_element_type=jnp.float32
    ).reshape(-1, model_width)
    shared_part = jnp.dot(shared_hidden, shared_down, preferred_element_type=jnp.float32)
    head_partial = jnp.dot(head_out, out_weight, preferred_element_type=jnp.float32)
    attn_sum, routed_sum, shared_sum = (
        summed_on_arrival(head_partial.astype(jnp.bfloat16), "tp", 0),
        summed_on_arrival(routed_part.astype(jnp.bfloat16), "tp", 0),
        summed_on_arrival(shared_part.astype(jnp.bfloat16), "tp", 0),
    )
    returned = lax.all_to_all(
        routed_sum.astype(jnp.bfloat16), EP, split_axis=0, concat_axis=0, tiled=True
    )
    combined = shared_sum
    for slot_pick in range(top_count):
        combined = combined + route_weights[:, slot_pick : slot_pick + 1] * jnp.take(
            returned, own_slots[:, slot_pick], axis=0
        ).astype(jnp.float32)
    return (attn_sum.astype(jnp.bfloat16), combined.astype(jnp.bfloat16))


def solution(mesh):
    torus = Mesh(
        mesh.devices.reshape(mesh.shape["grp"], 16, 2, mesh.shape["tp"]),
        ("grp", "ep_0", "ep_1", "tp"),
    )
    return jax.shard_map(
        body,
        mesh=torus,
        in_specs=(
            P(GRP_EP, "tp"),
            P(GRP_EP, "tp"),
            P(),
            P(),
            P("tp", None),
            P(GRP_EP_TP, None),
            P(),
            P(GRP_EP_TP, None),
            P(GRP_EP_TP, None),
            P(EP, None, "tp"),
            P(EP, None, "tp"),
            P(EP, "tp", None),
            P(None, "tp"),
            P(None, "tp"),
            P("tp", None),
        ),
        out_specs=(P(GRP_EP_TP, None), P(GRP_EP_TP, None)),
        check_vma=False,
    )
```

profile of v0, /device:TPU:33, one launch (start us, length us, event | category | flops | bytes accessed | tf_op | source)
XLA Modules:
  0.0 621.9 jit_solution(13244901644372939689)
XLA Ops:
  17.1 4.1 copy.120
  21.7 12.4 %reduce.10 = bf16[384,2048]{1,0:T(8,128)(2,1)} reduce(bf16[384,1,2048]{2,1,0:T(2,128)(2,1)} %bitcast.152, bf16[]{:T(256)} %broadcast.416), dimensions={1}, to_apply=%bitcast.134.reduce_sub_computation | reduce | bytes 3145730
  34.1 5.2 reshape.492
  39.3 25.6 %all-to-all-start.3 = ((bf16[32,2,12288]{2,1,0:T(2,128)(2,1)}), bf16[32,2,12288]{2,1,0:T(2,128)(2,1)}, u32[]{:S(2)}, u32[]{:S(2)}) async-start(bf16[32,2,12288]{2,1,0:T(2,128)(2,1)} %reshape.492), calls=%async_computation.3 | async-start | bytes 3145728 | tf_op jit(solution)/shard_map/all_to_all | solution.py:220
  66.8 95.3 %all-gather.8.cloned.1.call-done = bf16[6144,128]{0,1:T(8,128)(2,1)} async-done(((bf16[384,128]{0,1:T(8,128)(2,1)}), bf16[6144,128]{0,1:T(8,128)(2,1)}) %all-gather.8.cloned.1.call-update) | async-done | bytes 1572880 | tf_op jit(solution)/shard_map/all_gather | solution.py:24
  164.9 9.5 %reshape.493 = bf16[384,1,2048]{2,1,0:T(2,128)(2,1)} reshape(bf16[32,2,12288]{2,1,0:T(2,128)(2,1)} %all-to-all-done.3) | data formatting | bytes 3145728
  174.3 12.2 %bitcast_reduce_fusion.2 = bf16[384,2048]{1,0:T(8,128)(2,1)} fusion(bf16[384,1,2048]{2,1,0:T(2,128)(2,1)} %reshape.493), kind=kLoop, calls=%fused_computation.129 | loop fusion | bytes 3145728 | tf_op jit(solution)/shard_map/all_to_all | solution.py:220
  195.7 4.8 all-to-all-start.1
  202.6 25.4 %all-to-all-done.1 = bf16[4,128,2048]{2,1,0:T(8,128)(2,1)} async-done(((bf16[4,128,2048]{2,1,0:T(8,128)(2,1)}), bf16[4,128,2048]{2,1,0:T(8,128)(2,1)}, u32[]{:S(2)}, u32[]{:S(2)}) %all-to-all-start.1) | async-done | bytes 2097184 | tf_op jit(solution)/shard_map/all_to_all | solution.py:37
  230.3 5.5 convolution_convert_fusion
  235.8 4.5 all-to-all-start.2
  244.4 55.9 %all-gather.6.cloned.1.call-done = bf16[4,32,2,6,2048]{4,1,3,0,2:T(8,128)(2,1)} async-done(((bf16[1,32,2,6,2048]{4,1,3,0,2:T(8,128)(2,1)}), bf16[4,32,2,6,2048]{4,1,3,0,2:T(8,128)(2,1)}) %all-gather.6.cloned.1.call-update) | async-done | bytes 6291472 | tf_op jit(solution)/shard_map/all_gather | solution.py:223
  300.3 6.4 %fusion.14 = f32[2,4,32,6,256]{4,2,3,1,0:T(8,128)} fusion(bf16[4,32,2,6,2048]{4,1,3,0,2:T(8,128)(2,1)} %all-gather.6.cloned.1.call-done, bf16[2,2048,256]{2,1,0:T(8,128)(2,1)} %param.28), kind=kOutput, calls=%fused_computation.27 | convolution fusion | flops 1610612736 | bytes 9961472 | tf_op jit(solution)/shard_map/osjcd,jdf->osjcf/dot_general | solution.py:145
  306.7 10.1 %convert_bitcast_fusion = bf16[4,32,2,6,2048]{4,1,3,0,2:T(8,128)(2,1)} fusion(bf16[2,256,2048]{2,1,0:T(8,128)(2,1)S(1)} %copy-done, f32[2,4,32,6,256]{4,2,3,1,0:T(8,128)} %fusion.14, bf16[4,32,2,6,2048]{4,1,3,0,2:T(8,128)(2,1)} %all-gather.6.cloned.1.call-done, bf16[2,2048,256]{2,1,0:T(8,128)(2,1)} %param.29), kind=kOutput, calls=%fused_computation.20 | convolution fusion | flops 3226730496 | bytes 18350080 | tf_op jit(solution)/shard_map/osjcf,jfd->osjcd/dot_general | solution.py:225
  316.8 10.2 %copy.100 = bf16[4,32,2,6,2048]{4,0,3,2,1:T(4,128)(2,1)} copy(bf16[4,32,2,6,2048]{4,1,3,0,2:T(8,128)(2,1)} %convert_bitcast_fusion) | data formatting | bytes 12582912 | tf_op jit(solution)/shard_map/convert_element_type | solution.py:232
  327.0 9.1 %copy.101 = bf16[4,384,2048]{2,1,0:T(8,128)(2,1)} copy(bf16[4,384,2048]{2,0,1:T(4,128)(2,1)} %bitcast.151) | data formatting | bytes 12582912 | tf_op jit(solution)/shard_map/convert_element_type | solution.py:232
  336.1 5.3 all-to-all-start.4
  341.5 127.8 %while.15 = (s32[]{:T(128)}, f32[4,384]{1,0:T(4,128)S(1)}, f32[4,384]{1,0:T(4,128)S(1)}, f32[4,384,64]{1,2,0:T(8,128)S(1)}, bf16[12,1024,128]{2,1,0:T(8,128)(2,1...) while((s32[]{:T(128)}, f32[4,384]{1,0:T(4,128)S(1)}, f32[4,384]{1,0:T(4,128)S(1)}, ...), condition=%wide.region_5.6_spmd.clone, body=%wide.region_2.5_spmd.clone.sunk | while | flops 415538688 | bytes 46432384 | solution.py:134
  346.3 4.0 fusion.76
  357.0 4.0 fusion.76
  367.6 4.0 fusion.76
  378.2 4.0 fusion.76
  399.5 4.0 fusion.76
  420.8 4.0 fusion.76
  442.1 4.0 fusion.76
  463.4 4.0 fusion.76
  471.1 4.1 all-to-all-start
  475.3 5.7 reduce_sum.96
  484.5 10.4 %all-to-all-done = bf16[4,96,2048]{2,1,0:T(8,128)(2,1)S(1)} async-done(((bf16[4,96,2048]{2,1,0:T(8,128)(2,1)}), bf16[4,96,2048]{2,1,0:T(8,128)(2,1)S(1)}, u32[]{:S(2)}, u32[]{:S(2)}) %all-to-all-start) | async-done | bytes 1572896 | tf_op jit(solution)/shard_map/all_to_all | solution.py:52
  495.0 11.2 %all-to-all-start.5 = ((bf16[32,12,2048]{2,1,0:T(8,128)(2,1)}), bf16[32,12,2048]{2,1,0:T(8,128)(2,1)}, u32[]{:S(2)}, u32[]{:S(2)}) async-start(bf16[32,12,2048]{2,1,0:T(8,128)(2,1)} %all_to_all.28), calls=%async_computation.5 | async-start | bytes 4194304 | tf_op jit(solution)/shard_map/all_to_all | solution.py:235
  509.6 94.8 %all-to-all-done.5 = bf16[32,12,2048]{2,1,0:T(8,128)(2,1)} async-done(((bf16[32,12,2048]{2,1,0:T(8,128)(2,1)}), bf16[32,12,2048]{2,1,0:T(8,128)(2,1)}, u32[]{:S(2)}, u32[]{:S(2)}) %all-to-all-start.5) | async-done | bytes 1572896 | tf_op jit(solution)/shard_map/all_to_all | solution.py:235
  608.7 4.0 gather_fusion.2
  (212 shorter events, 143.3 us)
Async XLA Ops:
  7.2 299.5 %copy-start = (bf16[2,256,2048]{2,1,0:T(8,128)(2,1)S(1)}, bf16[2,256,2048]{2,1,0:T(8,128)(2,1)}, u32[]{:S(2)}) copy-start(bf16[2,256,2048]{2,1,0:T(8,128)(2,1)} %param.30) | copy-start | bytes 6291460
  39.3 25.7 %copy-start.5 = (bf16[384,128]{1,0:T(8,128)(2,1)S(1)}, bf16[384,128]{1,0:T(8,128)(2,1)}, u32[]{:S(2)}) copy-start(bf16[384,128]{1,0:T(8,128)(2,1)} %param.20) | copy-start | bytes 294916
  39.3 26.0 %copy-start.9 = (f32[64]{0:T(128)S(1)}, f32[64]{0:T(128)}, u32[]{:S(2)}) copy-start(f32[64]{0:T(128)} %param.22) | copy-start | bytes 772
  39.3 125.6 %all-to-all-start.3 = ((bf16[32,2,12288]{2,1,0:T(2,128)(2,1)}), bf16[32,2,12288]{2,1,0:T(2,128)(2,1)}, u32[]{:S(2)}, u32[]{:S(2)}) async-start(bf16[32,2,12288]{2,1,0:T(2,128)(2,1)} %reshape.492), calls=%async_computation.3 | async-start | bytes 3145728 | tf_op jit(solution)/shard_map/all_to_all | solution.py:220
  64.9 97.2 %all-gather.8.cloned.1.call-start = ((), (), s32[]{:S(2)}) async-start(), calls=%async_computation.7 | async-start | bytes 1671168 | tf_op jit(solution)/shard_map/all_gather | solution.py:24
  66.7 173.7 %all-gather.10.cloned.1.call-start = ((), (), s32[]{:S(2)}) async-start(), calls=%async_computation.8 | async-start | bytes 4718592 | tf_op jit(solution)/shard_map/all_gather | solution.py:24
  164.8 135.5 %all-gather.6.cloned.1.call-start = ((), (), s32[]{:S(2)}) async-start(), calls=%async_computation.6 | async-start | bytes 7864320 | tf_op jit(solution)/shard_map/all_gather | solution.py:223
  195.7 4.9 copy-start.6
  195.7 5.3 copy-start.10
  195.7 32.2 %all-to-all-start.1 = ((bf16[4,128,2048]{2,1,0:T(8,128)(2,1)}), bf16[4,128,2048]{2,1,0:T(8,128)(2,1)}, u32[]{:S(2)}, u32[]{:S(2)}) async-start(bf16[4,128,2048]{2,1,0:T(8,128)(2,1)} %broadcast_in_dim.47), calls=%async_computation.1 | async-start | bytes 4194304 | tf_op jit(solution)/shard_map/all_to_all | solution.py:37
  235.8 100.3 %all-to-all-start.2 = ((bf16[4,128,2048]{2,1,0:T(8,128)(2,1)}), bf16[4,128,2048]{2,1,0:T(8,128)(2,1)}, u32[]{:S(2)}, u32[]{:S(2)}) async-start(bf16[4,128,2048]{2,1,0:T(8,128)(2,1)} %bitcast.153), calls=%async_computation.2 | async-start | bytes 4194304 | tf_op jit(solution)/shard_map/all_to_all | solution.py:52
  336.1 135.0 %all-to-all-start.4 = ((bf16[4,384,2048]{2,1,0:T(8,128)(2,1)}), bf16[4,384,2048]{2,1,0:T(8,128)(2,1)}, u32[]{:S(2)}, u32[]{:S(2)}) async-start(bf16[4,384,2048]{2,1,0:T(8,128)(2,1)} %copy.101), calls=%async_computation.4 | async-start | bytes 12582912 | tf_op jit(solution)/shard_map/all_to_all | solution.py:52
  341.4 127.9 %copy-start.4 = (bf16[256,2048]{1,0:T(8,128)(2,1)S(1)}, bf16[256,2048]{1,0:T(8,128)(2,1)}, u32[]{:S(2)}) copy-start(bf16[256,2048]{1,0:T(8,128)(2,1)} %param.23) | copy-start | bytes 3145732
  346.3 4.6 copy-start.2
  357.0 4.6 copy-start.2
  367.6 4.6 copy-start.2
  378.2 4.6 copy-start.2
  388.9 4.6 copy-start.2
  399.5 4.6 copy-start.2
  410.2 4.6 copy-start.2
  420.8 4.6 copy-start.2
  431.5 4.6 copy-start.2
  442.1 4.6 copy-start.2
  452.7 4.6 copy-start.2
  463.4 4.6 copy-start.2
  471.1 23.9 %all-to-all-start = ((bf16[4,96,2048]{2,1,0:T(8,128)(2,1)}), bf16[4,96,2048]{2,1,0:T(8,128)(2,1)S(1)}, u32[]{:S(2)}, u32[]{:S(2)}) async-start(bf16[4,96,2048]{2,1,0:T(8,128)(2,1)} %bitcast.156), calls=%async_computation | async-start | bytes 3145728 | tf_op jit(solution)/shard_map/all_to_all | solution.py:52
  484.5 21.8 %copy-start.7 = (s32[128,2]{0,1:T(2,128)S(1)}, s32[128,2]{0,1:T(2,128)}, u32[]{:S(2)}) copy-start(s32[128,2]{0,1:T(2,128)} %param.26) | copy-start | bytes 3076
  484.5 21.9 %copy-start.8 = (f32[128,2]{0,1:T(2,128)S(1)}, f32[128,2]{0,1:T(2,128)}, u32[]{:S(2)}) copy-start(f32[128,2]{0,1:T(2,128)} %param.27) | copy-start | bytes 3076
  495.0 109.4 %all-to-all-start.5 = ((bf16[32,12,2048]{2,1,0:T(8,128)(2,1)}), bf16[32,12,2048]{2,1,0:T(8,128)(2,1)}, u32[]{:S(2)}, u32[]{:S(2)}) async-start(bf16[32,12,2048]{2,1,0:T(8,128)(2,1)} %all_to_all.28), calls=%async_computation.5 | async-start | bytes 4194304 | tf_op jit(solution)/shard_map/all_to_all | solution.py:235
  606.9 1.8 copy-start.3
  608.7 6.4 %copy-start.1 = (bf16[2,256,2048]{2,1,0:T(8,128)(2,1)S(1)}, bf16[2,256,2048]{2,1,0:T(8,128)(2,1)}, u32[]{:S(2)}) copy-start(bf16[2,256,2048]{2,1,0:T(8,128)(2,1)} %param.30) | copy-start | bytes 6291460
Sparse Core Ops, SparseCore 0:
  68.1 93.9 all-gather.7
  164.9 24.2 all-gather.9
  194.1 106.1 all-gather.5
where the time goes:
time: 626 us; the launch traced here: 622 us
  waiting for transfers between devices  282 us (45%)
  local copies, waits for them, and re-layouts  105 us (17%)
  matrix products  84.7 us (14%)
  other arithmetic  79.3 us (13%)
  starting transfers between devices  55.8 us (9%)
  between operations  14.5 us (2%)
    all_gather x2, waiting for transfers between devices, stacked_from(): tiles = lax.all_gather(tiles, axes[k])  95.4 us
    all_to_all x1, waiting for transfers between devices, body(): lax.all_to_all(routed_sum.astype(jnp.bfloat16), EP, split_axis=0, concat_...  94.8 us
    all_gather x1, waiting for transfers between devices, body(): lax.all_gather(arrived, 'tp', axis=0, tiled=True)  55.9 us
    reduce_sum x12, other arithmetic, one_block(): total_new = total_now * shrink + jnp.sum(exps, axis=-1)  47.6 us
    dot_general x12, matrix products, one_block(): jnp.einsum('qhd,kd->hqk', query_turned, block_rows[:, :head_size], prefer...  43.5 us
    all_to_all x1, starting transfers between devices, body(): lax.all_to_all(outgoing, EP, split_axis=1, concat_axis=1, tiled=True)  25.6 us
    all_to_all x1, waiting for transfers between devices, from_everyone(): return lax.all_to_all(copies, axis, split_axis=0, concat_axis=0, tiled=True)  25.4 us
    convert_element_type x2, local copies, waits for them, and re-layouts, body(): routed_part.astype(jnp.bfloat16)  19.3 us
  transfers between devices with their start and end apart: 9, of which 5 were waited for; matrix products, arithmetic and copies ran while one was open for 35% of the time, Pallas kernels for 0%

commit v1 on v0

--- a/solution.py
+++ b/solution.py
@@ -10,6 +10,11 @@
 GRP_EP_TP = ("grp", "ep_0", "ep_1", "tp")
 rope_base = 10000.0
 norm_eps = 1e-06
+
+
+def gather_by_exchange(value, axis, dim):
+    copies = jnp.concatenate([value] * lax.axis_size(axis), axis=dim)
+    return lax.all_to_all(copies, axis, dim, dim, tiled=True)
 
 
 def joined_along(tiles, dim):
@@ -219,9 +224,7 @@
     )[None]
     arrived = lax.all_to_all(outgoing, EP, split_axis=1, concat_axis=1, tiled=True)
     arrived = arrived.reshape(arrived.shape[0], ep_count, local_experts, capacity, model_width)
-    hidden = expert_hidden(
-        lax.all_gather(arrived, "tp", axis=0, tiled=True), expert_gate, expert_up
-    )
+    hidden = expert_hidden(gather_by_exchange(arrived, "tp", 0), expert_gate, expert_up)
     routed_part = jnp.einsum(
         "osjcf,jfd->osjcd", hidden, expert_down, preferred_element_type=jnp.float32
     ).reshape(-1, model_width)

time: 626 us -> 589 us (0.941)
  waiting for transfers between devices: 282 us -> 238 us
    all_to_all x1, waiting for transfers between devices: 0.01 us -> 77 us  [body(): lax.all_to_all(outgoing, EP, split_axis=1, concat_axis=1, tiled=True)]
    all_gather x2, waiting for transfers between devices: 95.4 us -> 35 us  [stacked_from(): tiles = lax.all_gather(tiles, axes[k])]
    all_gather x1 -> x0, waiting for transfers between devices: 55.9 us -> none  [body(): lax.all_gather(arrived, 'tp', axis=0, tiled=True)]
    all_to_all x1, waiting for transfers between devices: 25.4 us -> 0.01 us  [from_everyone(): return lax.all_to_all(copies, axis, split_axis=0, concat_axis=0, tiled=True)]
    all_to_all x0 -> x1, waiting for transfers between devices: none -> 19.2 us  [gather_by_exchange(): return lax.all_to_all(copies, axis, dim, dim, tiled=True)]
  transfers between devices with their start and end apart: 9 -> 9, of which waited for: 5 -> 6; matrix products, arithmetic and copies ran while one was open for 35% -> 37% of each run, Pallas kernels for 0% -> 0%
where the time goes in v1:
time: 589 us; the launch traced here: 584 us
  waiting for transfers between devices  238 us (40%)
  local copies, waits for them, and re-layouts  110 us (19%)
  matrix products  84.7 us (14%)
  other arithmetic  79.3 us (13%)
  starting transfers between devices  57.1 us (10%)
  between operations  14.7 us (2%)
    all_to_all x1, waiting for transfers between devices, body(): lax.all_to_all(routed_sum.astype(jnp.bfloat16), EP, split_axis=0, concat_...  96.8 us
    all_to_all x1, waiting for transfers between devices, body(): lax.all_to_all(outgoing, EP, split_axis=1, concat_axis=1, tiled=True)  77 us
    reduce_sum x12, other arithmetic, one_block(): total_new = total_now * shrink + jnp.sum(exps, axis=-1)  47.6 us
    dot_general x12, matrix products, one_block(): jnp.einsum('qhd,kd->hqk', query_turned, block_rows[:, :head_size], prefer...  43.5 us
    all_gather x2, waiting for transfers between devices, stacked_from(): tiles = lax.all_gather(tiles, axes[k])  35 us
    all_to_all x1, starting transfers between devices, body(): lax.all_to_all(outgoing, EP, split_axis=1, concat_axis=1, tiled=True)  25.6 us
    convert_element_type x2, local copies, waits for them, and re-layouts, body(): routed_part.astype(jnp.bfloat16)  19.3 us
    all_to_all x1, waiting for transfers between devices, gather_by_exchange(): return lax.all_to_all(copies, axis, dim, dim, tiled=True)  19.2 us
  transfers between devices with their start and end apart: 9, of which 6 were waited for; matrix products, arithmetic and copies ran while one was open for 37% of the time, Pallas kernels for 0%

profile of v1, /device:TPU:33, one launch (start us, length us, event | category | flops | bytes accessed | tf_op | source)
XLA Modules:
  0.0 584.1 jit_solution(6906188248415132187)
XLA Ops:
  17.1 4.1 copy.135
  21.7 12.4 %reduce.10 = bf16[384,2048]{1,0:T(8,128)(2,1)} reduce(bf16[384,1,2048]{2,1,0:T(2,128)(2,1)} %bitcast.150, bf16[]{:T(256)} %broadcast.417), dimensions={1}, to_apply=%bitcast.132.reduce_sub_computation | reduce | bytes 3145730
  34.1 5.0 reshape.494
  39.1 25.6 %all-to-all-start.3 = ((bf16[32,2,12288]{2,1,0:T(2,128)(2,1)}), bf16[32,2,12288]{2,1,0:T(2,128)(2,1)}, u32[]{:S(2)}, u32[]{:S(2)}) async-start(bf16[32,2,12288]{2,1,0:T(2,128)(2,1)} %reshape.494), calls=%async_computation.3 | async-start | bytes 3145728 | tf_op jit(solution)/shard_map/all_to_all | solution.py:225
  65.5 77.0 %all-to-all-done.3 = bf16[32,2,12288]{2,1,0:T(2,128)(2,1)} async-done(((bf16[32,2,12288]{2,1,0:T(2,128)(2,1)}), bf16[32,2,12288]{2,1,0:T(2,128)(2,1)}, u32[]{:S(2)}, u32[]{:S(2)}) %all-to-all-start.3) | async-done | bytes 1572896 | tf_op jit(solution)/shard_map/all_to_all | solution.py:225
  144.2 4.5 all-to-all-start.1
  149.7 9.5 %reshape.495 = bf16[384,1,2048]{2,1,0:T(2,128)(2,1)} reshape(bf16[32,2,12288]{2,1,0:T(2,128)(2,1)} %all-to-all-done.3) | data formatting | bytes 3145728
  159.2 12.2 %bitcast_reduce_fusion.2 = bf16[384,2048]{1,0:T(8,128)(2,1)} fusion(bf16[384,1,2048]{2,1,0:T(2,128)(2,1)} %reshape.495), kind=kLoop, calls=%fused_computation.131 | loop fusion | bytes 3145728 | tf_op jit(solution)/shard_map/all_to_all | solution.py:225
  171.5 4.1 reshape.452
  179.2 4.9 concatenate.45
  184.1 5.3 all-to-all-start.4
  189.5 16.3 %all-gather.5.cloned.1.call-done = bf16[6144,128]{0,1:T(8,128)(2,1)} async-done(((bf16[384,128]{0,1:T(8,128)(2,1)}), bf16[6144,128]{0,1:T(8,128)(2,1)}) %all-gather.5.cloned.1.call-update) | async-done | bytes 1572880 | tf_op jit(solution)/shard_map/all_gather | solution.py:29
  212.9 5.5 convolution_convert_fusion
  218.4 18.7 %all-gather.7.cloned.1.call-done = bf16[32,384,128]{2,1,0:T(8,128)(2,1)} async-done(((bf16[16,384,128]{2,1,0:T(8,128)(2,1)}), bf16[32,384,128]{2,1,0:T(8,128)(2,1)}) %all-gather.7.cloned.1.call-update) | async-done | bytes 3145744 | tf_op jit(solution)/shard_map/all_gather | solution.py:29
  241.0 19.2 %all-to-all-done.4 = bf16[4,32,2,6,2048]{4,1,3,2,0:T(8,128)(2,1)} async-done(((bf16[4,32,2,6,2048]{4,1,3,2,0:T(8,128)(2,1)}), bf16[4,32,2,6,2048]{4,1,3,2,0:T(8,128)(2,1)}, u32[]{:S(2)}, u32[]{:S(2)}) %all-to-all-start.4) | async-done | bytes 6291488 | tf_op jit(solution)/shard_map/all_to_all | solution.py:17
  260.2 4.7 all-to-all-start.2
  265.0 6.4 %fusion.13 = f32[2,4,32,6,256]{4,2,3,1,0:T(8,128)} fusion(bf16[4,32,2,6,2048]{4,1,3,2,0:T(8,128)(2,1)} %all-to-all-done.4, bf16[2,2048,256]{2,1,0:T(8,128)(2,1)} %param.28), kind=kOutput, calls=%fused_computation.23 | convolution fusion | flops 1610612736 | bytes 9961472 | tf_op jit(solution)/shard_map/osjcd,jdf->osjcf/dot_general | solution.py:150
  271.4 10.1 %convert_bitcast_fusion = bf16[4,32,2,6,2048]{4,1,3,0,2:T(8,128)(2,1)} fusion(bf16[2,256,2048]{2,1,0:T(8,128)(2,1)S(1)} %copy-done, f32[2,4,32,6,256]{4,2,3,1,0:T(8,128)} %fusion.13, bf16[2,2048,256]{2,1,0:T(8,128)(2,1)} %param.29, bf16[4,32,2,6,2048]{4,1,3,2,0:T(8,128)(2,1)} %all-to-all-done.4), kind=kOutput, calls=%fused_computation.20 | convolution fusion | flops 3226730496 | bytes 18350080 | tf_op jit(solution)/shard_map/osjcf,jfd->osjcd/dot_general | solution.py:228
  281.4 10.2 %copy.107 = bf16[4,32,2,6,2048]{4,0,3,2,1:T(4,128)(2,1)} copy(bf16[4,32,2,6,2048]{4,1,3,0,2:T(8,128)(2,1)} %convert_bitcast_fusion) | data formatting | bytes 12582912 | tf_op jit(solution)/shard_map/convert_element_type | solution.py:235
  291.7 9.1 %copy.108 = bf16[4,384,2048]{2,1,0:T(8,128)(2,1)} copy(bf16[4,384,2048]{2,0,1:T(4,128)(2,1)} %bitcast.149) | data formatting | bytes 12582912 | tf_op jit(solution)/shard_map/convert_element_type | solution.py:235
  300.8 5.3 all-to-all-start.5
  306.1 127.8 %while.15 = (s32[]{:T(128)}, f32[4,384]{1,0:T(4,128)S(1)}, f32[4,384]{1,0:T(4,128)S(1)}, f32[4,384,64]{1,2,0:T(8,128)S(1)}, bf16[12,1024,128]{2,1,0:T(8,128)(2,1...) while((s32[]{:T(128)}, f32[4,384]{1,0:T(4,128)S(1)}, f32[4,384]{1,0:T(4,128)S(1)}, ...), condition=%wide.region_5.6_spmd.clone, body=%wide.region_2.5_spmd.clone.sunk | while | flops 415538688 | bytes 46432384 | solution.py:139
  311.0 4.0 fusion.80
  364.2 4.0 fusion.80
  385.5 4.0 fusion.80
  406.8 4.0 fusion.80
  435.8 4.1 all-to-all-start
  439.9 5.7 reduce_sum.96
  449.2 9.6 %all-to-all-done = bf16[4,96,2048]{2,1,0:T(8,128)(2,1)S(1)} async-done(((bf16[4,96,2048]{2,1,0:T(8,128)(2,1)}), bf16[4,96,2048]{2,1,0:T(8,128)(2,1)S(1)}, u32[]{:S(2)}, u32[]{:S(2)}) %all-to-all-start) | async-done | bytes 1572896 | tf_op jit(solution)/shard_map/all_to_all | solution.py:57
  458.8 7.3 %all-to-all-start.6 = ((bf16[32,12,2048]{2,1,0:T(8,128)(2,1)}), bf16[32,12,2048]{2,1,0:T(8,128)(2,1)}, u32[]{:S(2)}, u32[]{:S(2)}) async-start(bf16[32,12,2048]{2,1,0:T(8,128)(2,1)} %all_to_all.32), calls=%async_computation.6 | async-start | bytes 4194304 | tf_op jit(solution)/shard_map/all_to_all | solution.py:238
  469.6 96.8 %all-to-all-done.6 = bf16[32,12,2048]{2,1,0:T(8,128)(2,1)} async-done(((bf16[32,12,2048]{2,1,0:T(8,128)(2,1)}), bf16[32,12,2048]{2,1,0:T(8,128)(2,1)}, u32[]{:S(2)}, u32[]{:S(2)}) %all-to-all-start.6) | async-done | bytes 1572896 | tf_op jit(solution)/shard_map/all_to_all | solution.py:238
  570.6 4.0 gather_fusion.2
  (212 shorter events, 155.2 us)
Async XLA Ops:
  7.2 264.2 %copy-start = (bf16[2,256,2048]{2,1,0:T(8,128)(2,1)S(1)}, bf16[2,256,2048]{2,1,0:T(8,128)(2,1)}, u32[]{:S(2)}) copy-start(bf16[2,256,2048]{2,1,0:T(8,128)(2,1)} %param.30) | copy-start | bytes 6291460
  39.1 25.6 %copy-start.5 = (bf16[384,128]{1,0:T(8,128)(2,1)S(1)}, bf16[384,128]{1,0:T(8,128)(2,1)}, u32[]{:S(2)}) copy-start(bf16[384,128]{1,0:T(8,128)(2,1)} %param.20) | copy-start | bytes 294916
  39.1 25.9 %copy-start.9 = (f32[64]{0:T(128)S(1)}, f32[64]{0:T(128)}, u32[]{:S(2)}) copy-start(f32[64]{0:T(128)} %param.22) | copy-start | bytes 772
  39.1 103.5 %all-to-all-start.3 = ((bf16[32,2,12288]{2,1,0:T(2,128)(2,1)}), bf16[32,2,12288]{2,1,0:T(2,128)(2,1)}, u32[]{:S(2)}, u32[]{:S(2)}) async-start(bf16[32,2,12288]{2,1,0:T(2,128)(2,1)} %reshape.494), calls=%async_computation.3 | async-start | bytes 3145728 | tf_op jit(solution)/shard_map/all_to_all | solution.py:225
  144.2 34.9 %all-to-all-start.1 = ((bf16[4,128,2048]{2,1,0:T(8,128)(2,1)}), bf16[4,128,2048]{2,1,0:T(8,128)(2,1)}, u32[]{:S(2)}, u32[]{:S(2)}) async-start(bf16[4,128,2048]{2,1,0:T(8,128)(2,1)} %broadcast_in_dim.47), calls=%async_computation.1 | async-start | bytes 4194304 | tf_op jit(solution)/shard_map/all_to_all | solution.py:42
  148.8 57.0 %all-gather.5.cloned.1.call-start = ((), (), s32[]{:S(2)}) async-start(), calls=%async_computation.7 | async-start | bytes 1671168 | tf_op jit(solution)/shard_map/all_gather | solution.py:29
  184.1 76.2 %all-to-all-start.4 = ((bf16[4,32,2,6,2048]{4,1,3,2,0:T(8,128)(2,1)}), bf16[4,32,2,6,2048]{4,1,3,2,0:T(8,128)(2,1)}, u32[]{:S(2)}, u32[]{:S(2)}) async-start(bf16[4,32,2,6,2048]{4,1,3,2,0:T(8,128)(2,1)} %concatenate.45), calls=%async_computation.4 | async-start | bytes 12582912 | tf_op jit(solution)/shard_map/all_to_all | solution.py:17
  189.4 19.1 %copy-start.6 = (bf16[384,256]{1,0:T(8,128)(2,1)S(1)}, bf16[384,256]{1,0:T(8,128)(2,1)}, u32[]{:S(2)}) copy-start(bf16[384,256]{1,0:T(8,128)(2,1)} %param.19) | copy-start | bytes 589828
  189.4 19.5 %copy-start.10 = (f32[64]{0:T(128)S(1)}, f32[64]{0:T(128)}, u32[]{:S(2)}) copy-start(f32[64]{0:T(128)} %param.21) | copy-start | bytes 772
  189.4 47.7 %all-gather.7.cloned.1.call-start = ((), (), s32[]{:S(2)}) async-start(), calls=%async_computation.8 | async-start | bytes 4718592 | tf_op jit(solution)/shard_map/all_gather | solution.py:29
  260.2 40.6 %all-to-all-start.2 = ((bf16[4,128,2048]{2,1,0:T(8,128)(2,1)}), bf16[4,128,2048]{2,1,0:T(8,128)(2,1)}, u32[]{:S(2)}, u32[]{:S(2)}) async-start(bf16[4,128,2048]{2,1,0:T(8,128)(2,1)} %bitcast.151), calls=%async_computation.2 | async-start | bytes 4194304 | tf_op jit(solution)/shard_map/all_to_all | solution.py:57
  300.8 135.0 %all-to-all-start.5 = ((bf16[4,384,2048]{2,1,0:T(8,128)(2,1)}), bf16[4,384,2048]{2,1,0:T(8,128)(2,1)}, u32[]{:S(2)}, u32[]{:S(2)}) async-start(bf16[4,384,2048]{2,1,0:T(8,128)(2,1)} %copy.108), calls=%async_computation.5 | async-start | bytes 12582912 | tf_op jit(solution)/shard_map/all_to_all | solution.py:57
  306.1 127.9 %copy-start.4 = (bf16[256,2048]{1,0:T(8,128)(2,1)S(1)}, bf16[256,2048]{1,0:T(8,128)(2,1)}, u32[]{:S(2)}) copy-start(bf16[256,2048]{1,0:T(8,128)(2,1)} %param.23) | copy-start | bytes 3145732
  311.0 4.6 copy-start.2
  321.6 4.6 copy-start.2
  332.3 4.6 copy-start.2
  342.9 4.6 copy-start.2
  353.6 4.6 copy-start.2
  364.2 4.6 copy-start.2
  374.9 4.6 copy-start.2
  385.5 4.6 copy-start.2
  396.1 4.6 copy-start.2
  406.8 4.6 copy-start.2
  417.4 4.6 copy-start.2
  428.1 4.6 copy-start.2
  435.8 23.0 %all-to-all-start = ((bf16[4,96,2048]{2,1,0:T(8,128)(2,1)}), bf16[4,96,2048]{2,1,0:T(8,128)(2,1)S(1)}, u32[]{:S(2)}, u32[]{:S(2)}) async-start(bf16[4,96,2048]{2,1,0:T(8,128)(2,1)} %bitcast.154), calls=%async_computation | async-start | bytes 3145728 | tf_op jit(solution)/shard_map/all_to_all | solution.py:57
  449.2 17.1 %copy-start.7 = (s32[128,2]{0,1:T(2,128)S(1)}, s32[128,2]{0,1:T(2,128)}, u32[]{:S(2)}) copy-start(s32[128,2]{0,1:T(2,128)} %param.26) | copy-start | bytes 3076
  449.2 17.2 %copy-start.8 = (f32[128,2]{0,1:T(2,128)S(1)}, f32[128,2]{0,1:T(2,128)}, u32[]{:S(2)}) copy-start(f32[128,2]{0,1:T(2,128)} %param.27) | copy-start | bytes 3076
  458.8 107.6 %all-to-all-start.6 = ((bf16[32,12,2048]{2,1,0:T(8,128)(2,1)}), bf16[32,12,2048]{2,1,0:T(8,128)(2,1)}, u32[]{:S(2)}, u32[]{:S(2)}) async-start(bf16[32,12,2048]{2,1,0:T(8,128)(2,1)} %all_to_all.32), calls=%async_computation.6 | async-start | bytes 4194304 | tf_op jit(solution)/shard_map/all_to_all | solution.py:238
  568.9 1.8 copy-start.3
  570.6 6.4 %copy-start.1 = (bf16[2,256,2048]{2,1,0:T(8,128)(2,1)S(1)}, bf16[2,256,2048]{2,1,0:T(8,128)(2,1)}, u32[]{:S(2)}) copy-start(bf16[2,256,2048]{2,1,0:T(8,128)(2,1)} %param.30) | copy-start | bytes 6291460
Sparse Core Ops, SparseCore 0:
  152.0 53.7 all-gather.4
  208.6 28.4 all-gather.6
